TPU v7x, 32 devices: a whole 2x2x4 slice. The times are simulated.
32 devices in a mesh: sp: 8 (over z, x), tp: 4 (over y, core).
Axes of the slice: x: 2, y: 2, z: 4, core: 2. Of those that a mesh axis runs over, the one named last changes fastest.
Arguments:
- stream: bfloat16 [4096, 2048], P('sp', 'tp'), may hold values from -6 to 6
- norm_gain: float32 [2, 2048], replicated, may hold values from 0.1 to 1.9
- w_value: bfloat16 [2, 2048, 2048], P(None, 'sp', 'tp'), may hold values from -0.125 to 0.125
- w_inner: bfloat16 [2, 2048, 2048], P(None, 'sp', 'tp'), may hold values from -0.125 to 0.125
- w_outer: bfloat16 [2, 2048, 2048], P(None, 'sp', 'tp'), may hold values from -0.125 to 0.125
- conv_taps: float32 [2, 3, 2048], P(None, None, 'tp'), may hold values from -3 to 3
- w_output: bfloat16 [2, 2048, 2048], P(None, 'tp', 'sp'), may hold values from -0.125 to 0.125
Outputs:
- result: bfloat16 [4096, 2048], P('sp', 'tp')
All inputs are finite; a program needn't handle non-finite values.
Results may differ from a plain program's by a relative error of at most 0.02.
Values may be sent and summed in bfloat16 or wider, within the bound.
A program may use at most 64 MiB of HBM per device.

v0:
```python
import jax
import jax.numpy as jnp
from jax import lax
from jax.sharding import PartitionSpec as P

LAYERS = 2
EPSILON = 1e-06


def passed_along(block, axis, distance):
    devices = range(lax.axis_size(axis))
    route = [(i - distance, i) for i in devices if i - distance in devices]
    return lax.ppermute(block, axis, route)


def on_device(stream, norm_gain, w_value, w_inner, w_outer, conv_taps, w_output):
    gathered_in = (
        lax.all_gather(w_value, "sp", axis=1, tiled=True),
        lax.all_gather(w_inner, "sp", axis=1, tiled=True),
        lax.all_gather(w_outer, "sp", axis=1, tiled=True),
    )
    gathered_out = lax.all_gather(w_output, "sp", axis=2, tiled=True)
    stream_now = stream
    for layer_index in range(LAYERS):
        layer_value = gathered_in[0][layer_index]
        layer_inner = gathered_in[1][layer_index]
        layer_outer = gathered_in[2][layer_index]
        layer_output = gathered_out[layer_index]
        full_rows = lax.all_gather(stream_now, "tp", axis=1, tiled=True)
        row_float = full_rows.astype(jnp.float32)
        scale = lax.rsqrt(jnp.mean(row_float * row_float, axis=-1, keepdims=True) + EPSILON)
        normed = (row_float * scale * norm_gain[layer_index]).astype(jnp.bfloat16)
        row_count = normed.shape[0]
        value_proj = jnp.dot(normed, layer_value, preferred_element_type=jnp.float32)
        inner_gate = jnp.dot(normed, layer_inner, preferred_element_type=jnp.float32)
        outer_gate = jnp.dot(normed, layer_outer, preferred_element_type=jnp.float32)
        mixed = (inner_gate * value_proj).astype(jnp.bfloat16)
        before = passed_along(mixed[row_count - 2 :], "sp", 1)
        padded = jnp.concatenate([before, mixed], axis=0).astype(jnp.float32)
        taps = conv_taps[layer_index]
        convolved = (
            taps[0] * padded[0:row_count]
            + taps[1] * padded[1 : row_count + 1]
            + taps[2] * padded[2:]
        )
        gated = (outer_gate * convolved).astype(jnp.bfloat16)
        terms = jnp.dot(gated, layer_output, preferred_element_type=jnp.float32).astype(
            jnp.bfloat16
        )
        summed = lax.psum_scatter(
            terms.astype(jnp.float32).astype(jnp.bfloat16), "tp", scatter_dimension=1, tiled=True
        ).astype(jnp.float32)
        stream_now = (stream_now.astype(jnp.float32) + summed).astype(jnp.bfloat16)
    return stream_now


def solution(mesh):
    in_specs = (
        P("sp", "tp"),
        P(),
        P(None, "sp", "tp"),
        P(None, "sp", "tp"),
        P(None, "sp", "tp"),
        P(None, None, "tp"),
        P(None, "tp", "sp"),
    )
    out_specs = P("sp", "tp")
    return jax.shard_map(
        on_device, mesh=mesh, in_specs=in_specs, out_specs=out_specs, check_vma=False
    )
```

profile of v0, /device:TPU:0, one launch (start us, length us, event | category | flops | bytes accessed | tf_op | source)
XLA Modules:
  0.0 450.2 jit_solution(300876081806969072)
XLA Ops:
  6.5 0.7 all-gather.7.cloned.1.call-update
  7.3 0.7 all-gather.13.cloned.1.call-update
  8.1 0.7 all-gather.11.cloned.1.call-update
  8.8 0.5 all-gather.9.cloned.1.call-update
  9.4 0.5 all-gather.15.cloned.1.call-update
  9.9 0.0 reduce-scatter.3.cloned.1.call-start
  10.0 24.2 %all-gather.7.cloned.1.call-done = bf16[512,2048]{1,0:T(8,128)(2,1)} async-done(((bf16[512,512]{1,0:T(8,128)(2,1)}), bf16[512,2048]{1,0:T(8,128)(2,1)}) %all-gather.7.cloned.1.call-update) | async-done | bytes 2097168 | tf_op jit(solution)/shard_map/all_gather | solution.py:29
  34.2 2.2 fusion
  36.5 72.7 %all-gather.13.cloned.1.call-done = bf16[2,2048,512]{2,1,0:T(8,128)(2,1)} async-done(((bf16[2,256,512]{2,1,0:T(8,128)(2,1)}), bf16[2,2048,512]{2,1,0:T(8,128)(2,1)}) %all-gather.13.cloned.1.call-update) | async-done | bytes 4194320 | tf_op jit(solution)/shard_map/all_gather | solution.py:18
  109.2 2.9 fusion.9
  112.1 70.6 %all-gather.11.cloned.1.call-done = bf16[2,2048,512]{2,1,0:T(8,128)(2,1)} async-done(((bf16[2,256,512]{2,1,0:T(8,128)(2,1)}), bf16[2,2048,512]{2,1,0:T(8,128)(2,1)}) %all-gather.11.cloned.1.call-update) | async-done | bytes 4194320 | tf_op jit(solution)/shard_map/all_gather | solution.py:19
  182.7 2.9 fusion.18
  185.6 2.5 collective-permute-start
  188.1 1.3 collective-permute-done
  189.4 0.2 maximum_convert_fusion
  189.6 66.6 %all-gather.9.cloned.1.call-done = bf16[2,2048,512]{2,1,0:T(8,128)(2,1)} async-done(((bf16[2,256,512]{2,1,0:T(8,128)(2,1)}), bf16[2,2048,512]{2,1,0:T(8,128)(2,1)}) %all-gather.9.cloned.1.call-update) | async-done | bytes 4194320 | tf_op jit(solution)/shard_map/all_gather | solution.py:20
  256.1 75.1 %all-gather.15.cloned.1.call-done = bf16[2,512,2048]{2,1,0:T(8,128)(2,1)} async-done(((bf16[2,512,256]{2,1,0:T(8,128)(2,1)}), bf16[2,512,2048]{2,1,0:T(8,128)(2,1)}) %all-gather.15.cloned.1.call-update) | async-done | bytes 4194320 | tf_op jit(solution)/shard_map/all_gather | solution.py:22
  331.2 6.1 %convolution_convert_fusion.1 = bf16[512,2048]{1,0:T(8,128)(2,1)} fusion(bf16[2,512,2048]{2,1,0:T(8,128)(2,1)} %all-gather.15.cloned.1.call-done, bf16[2,2048,512]{2,1,0:T(8,128)(2,1)} %all-gather.9.cloned.1.call-done, f32[514,512]{1,0:T(8,128)S(1)} %maximum_convert_fusion, f32[512]{0:T(512)S(1)} %bitcast.61, f32[512]{0:T(512)S(1)} %bitcast.62, ...), kind=kOutput, calls=%fused_computation.11 | convolution fusion | flops 2154561536 | bytes 11550720 | tf_op jit(solution)/shard_map/dot_general | solution.py:47
  337.3 0.0 all-gather.17.cloned.1.call-start
  337.4 29.5 %reduce-scatter.3.cloned.1.call-done = bf16[512,512]{1,0:T(8,128)(2,1)} async-done(((bf16[512,2048]{1,0:T(8,128)(2,1)}), bf16[512,512]{1,0:T(8,128)(2,1)}) %reduce-scatter.3.cloned.1.call-update) | async-done | bytes 524304 | tf_op jit(solution)/shard_map/reduce_scatter | solution.py:50
  366.9 2.0 add_convert_fusion.1
  368.9 0.0 reduce-scatter.5.cloned.1.call-start
  368.9 22.6 %all-gather.17.cloned.1.call-done = bf16[512,2048]{1,0:T(8,128)(2,1)} async-done(((bf16[512,512]{1,0:T(8,128)(2,1)}), bf16[512,2048]{1,0:T(8,128)(2,1)}) %all-gather.17.cloned.1.call-update) | async-done | bytes 2097168 | tf_op jit(solution)/shard_map/all_gather | solution.py:29
  391.6 2.2 fusion.3
  393.8 3.0 fusion.6
  396.9 1.3 fusion.16
  398.2 3.4 collective-permute-start.1
  401.6 1.3 collective-permute-done.1
  402.8 0.2 maximum_convert_fusion.1
  403.0 6.2 %convolution_convert_fusion = bf16[512,2048]{1,0:T(8,128)(2,1)} fusion(bf16[2,512,2048]{2,1,0:T(8,128)(2,1)} %all-gather.15.cloned.1.call-done, bf16[2,2048,512]{2,1,0:T(8,128)(2,1)} %all-gather.9.cloned.1.call-done, f32[514,512]{1,0:T(8,128)S(1)} %maximum_convert_fusion.1, f32[512]{0:T(512)S(1)} %bitcast.59, f32[512]{0:T(512)S(1)} %bitcast.60, ...), kind=kOutput, calls=%fused_computation.10 | convolution fusion | flops 2154561536 | bytes 11550720 | tf_op jit(solution)/shard_map/dot_general | solution.py:47
  409.2 32.1 %reduce-scatter.5.cloned.1.call-done = bf16[512,512]{1,0:T(8,128)(2,1)} async-done(((bf16[512,2048]{1,0:T(8,128)(2,1)}), bf16[512,512]{1,0:T(8,128)(2,1)}) %reduce-scatter.5.cloned.1.call-update) | async-done | bytes 524304 | tf_op jit(solution)/shard_map/reduce_scatter | solution.py:50
  441.4 2.0 add_convert_fusion
  (28 shorter events, 0.3 us)
Async XLA Ops:
  6.5 3.4 copy-start.4
  6.5 27.7 %all-gather.7.cloned.1.call-start = ((), (), s32[]{:S(2)}) async-start(), calls=%async_computation.2 | async-start | bytes 2621440 | tf_op jit(solution)/shard_map/all_gather | solution.py:29
  7.3 101.9 %all-gather.13.cloned.1.call-start = ((), (), s32[]{:S(2)}) async-start(), calls=%async_computation.5 | async-start | bytes 4718592 | tf_op jit(solution)/shard_map/all_gather | solution.py:18
  8.0 174.7 %all-gather.11.cloned.1.call-start = ((), (), s32[]{:S(2)}) async-start(), calls=%async_computation.4 | async-start | bytes 4718592 | tf_op jit(solution)/shard_map/all_gather | solution.py:19
  8.7 247.4 %all-gather.9.cloned.1.call-start = ((), (), s32[]{:S(2)}) async-start(), calls=%async_computation.3 | async-start | bytes 4718592 | tf_op jit(solution)/shard_map/all_gather | solution.py:20
  9.3 321.9 %all-gather.15.cloned.1.call-start = ((), (), s32[]{:S(2)}) async-start(), calls=%async_computation.6 | async-start | bytes 4718592 | tf_op jit(solution)/shard_map/all_gather | solution.py:22
  9.9 357.0 %reduce-scatter.3.cloned.1.call-start = ((), (), s32[]{:S(2)}) async-start(), calls=%async_computation.7 | async-start | bytes 2621440 | tf_op jit(solution)/shard_map/reduce_scatter | solution.py:50
  34.2 75.0 %copy-start.2 = (bf16[512,2048]{1,0:T(8,128)(2,1)S(1)}, bf16[512,2048]{1,0:T(8,128)(2,1)}, u32[]{:S(2)}) copy-start(bf16[512,2048]{1,0:T(8,128)(2,1)} %all-gather.7.cloned.1.call-done) | copy-start | bytes 6291460
  112.1 76.0 %copy-start.5 = (f32[2,3,512]{2,0,1:T(2,128)S(1)}, f32[2,3,512]{2,0,1:T(2,128)}, u32[]{:S(2)}) copy-start(f32[2,3,512]{2,0,1:T(2,128)} %param.12) | copy-start | bytes 36868
  185.6 3.8 collective-permute-start
  337.3 29.5 %copy-start.1 = (bf16[512,512]{1,0:T(8,128)(2,1)S(1)}, bf16[512,512]{1,0:T(8,128)(2,1)}, u32[]{:S(2)}) copy-start(bf16[512,512]{1,0:T(8,128)(2,1)} %param.7) | copy-start | bytes 1572868
  337.3 54.2 %all-gather.17.cloned.1.call-start = ((), (), s32[]{:S(2)}) async-start(), calls=%async_computation.8 | async-start | bytes 2621440 | tf_op jit(solution)/shard_map/all_gather | solution.py:29
  368.9 72.5 %reduce-scatter.5.cloned.1.call-start = ((), (), s32[]{:S(2)}) async-start(), calls=%async_computation.9 | async-start | bytes 2621440 | tf_op jit(solution)/shard_map/reduce_scatter | solution.py:50
  391.6 2.2 copy-start.3
  393.8 3.0 copy-start.6
  398.2 4.7 %collective-permute-start.1 = (bf16[2,512]{1,0:T(2,128)(2,1)S(1)}, bf16[2,512]{1,0:T(2,128)(2,1)S(1)}, u32[]{:S(2)}, u32[]{:S(2)}) collective-permute-start(bf16[2,512]{1,0:T(2,128)(2,1)S(1)} %slice.121), channel_id=1, source_target_pairs={{0,4},{4,8},{8,12},{12,16},{16,20},{20,24},{24,28},{1,5},{5,9},{9,... | collective-permute-start | bytes 6152 | tf_op jit(solution)/shard_map/ppermute | solution.py:13
  409.2 32.2 %copy-start = (bf16[512,512]{1,0:T(8,128)(2,1)S(1)}, bf16[512,512]{1,0:T(8,128)(2,1)}, u32[]{:S(2)}) copy-start(bf16[512,512]{1,0:T(8,128)(2,1)} %add_convert_fusion.1) | copy-start | bytes 1572868
Sparse Core Ops, SparseCore 0:
  8.9 25.2 all-gather.6
  36.4 72.7 all-gather.12
  111.4 71.2 all-gather.10
  184.8 71.2 all-gather.8
  258.0 73.1 all-gather.14
  337.5 29.3 reduce-scatter.2
  369.0 22.5 all-gather.16
  409.3 31.9 reduce-scatter.4
where the time goes:
time: 450 us
  waiting for transfers between devices  399 us (89%)
  matrix products  22.4 us (5%)
  between operations  13.6 us (3%)
  other arithmetic  8.7 us (2%)
  starting transfers between devices  6.12 us (1%)
    all_gather x1, waiting for transfers between devices, on_device(): gathered_out = lax.all_gather(w_output, 'sp', axis=2, tiled=True)  75.1 us
    all_gather x1, waiting for transfers between devices, on_device(): lax.all_gather(w_value, 'sp', axis=1, tiled=True)  72.7 us
    all_gather x1, waiting for transfers between devices, on_device(): lax.all_gather(w_inner, 'sp', axis=1, tiled=True)  70.6 us
    all_gather x1, waiting for transfers between devices, on_device(): lax.all_gather(w_outer, 'sp', axis=1, tiled=True)  66.6 us
    reduce_scatter x2, waiting for transfers between devices, on_device(): lax.psum_scatter(terms.astype(jnp.float32).astype(jnp.bfloat16), 'tp', sc...  61.6 us
    all_gather x2, waiting for transfers between devices, on_device(): full_rows = lax.all_gather(stream_now, 'tp', axis=1, tiled=True)  46.9 us
    dot_general x2, matrix products, on_device(): jnp.dot(gated, layer_output, preferred_element_type=jnp.float32)  12.3 us
  transfers between devices with their start and end apart: 10, of which 10 were waited for; matrix products, arithmetic and copies ran while one was open for 2% of the time, Pallas kernels for 0%

commit v1 on v0

--- a/solution.py
+++ b/solution.py
@@ -26,7 +26,14 @@
         layer_inner = gathered_in[1][layer_index]
         layer_outer = gathered_in[2][layer_index]
         layer_output = gathered_out[layer_index]
-        full_rows = lax.all_gather(stream_now, "tp", axis=1, tiled=True)
+        ring = [stream_now]
+        for hop in range(3):
+            ring.append(lax.ppermute(ring[-1], "tp", [(dev, (dev + 1) % 4) for dev in range(4)]))
+        full_rows = jnp.roll(
+            jnp.concatenate(ring[::-1], axis=1),
+            (lax.axis_index("tp") + 1) * ring[0].shape[1],
+            axis=1,
+        )
         row_float = full_rows.astype(jnp.float32)
         scale = lax.rsqrt(jnp.mean(row_float * row_float, axis=-1, keepdims=True) + EPSILON)
         normed = (row_float * scale * norm_gain[layer_index]).astype(jnp.bfloat16)

time: 450 us -> 435 us (0.967)
  waiting for transfers between devices: 399 us -> 371 us
  other arithmetic: 8.7 us -> 17.1 us
    ppermute x0 -> x6, waiting for transfers between devices: none -> 51.3 us  [on_device(): lax.ppermute(ring[-1], 'tp', [(dev, (dev + 1) % 4) for dev in range(4)])]
    all_gather x2 -> x0, waiting for transfers between devices: 46.9 us -> none  [on_device(): full_rows = lax.all_gather(stream_now, 'tp', axis=1, tiled=True)]
    all_gather x1, waiting for transfers between devices: 72.7 us -> 43 us  [on_device(): lax.all_gather(w_value, 'sp', axis=1, tiled=True)]
    reduce_sum x2, other arithmetic: 4.45 us -> 11.5 us  [on_device(): jnp.mean(row_float * row_float, axis=-1, keepdims=True) + EPSILON]
  transfers between devices with their start and end apart: 10 -> 14, of which waited for: 10 -> 14; matrix products, arithmetic and copies ran while one was open for 2% -> 3% of each run, Pallas kernels for 0% -> 0%
where the time goes in v1:
time: 435 us; the launch traced here: 434 us
  waiting for transfers between devices  371 us (85%)
  matrix products  23.9 us (5%)
  other arithmetic  17.1 us (4%)
  between operations  13.6 us (3%)
  starting transfers between devices  6.68 us (2%)
    all_gather x1, waiting for transfers between devices, on_device(): gathered_out = lax.all_gather(w_output, 'sp', axis=2, tiled=True)  75.1 us
    all_gather x1, waiting for transfers between devices, on_device(): lax.all_gather(w_inner, 'sp', axis=1, tiled=True)  69.6 us
    all_gather x1, waiting for transfers between devices, on_device(): lax.all_gather(w_outer, 'sp', axis=1, tiled=True)  65.5 us
    reduce_scatter x2, waiting for transfers between devices, on_device(): lax.psum_scatter(terms.astype(jnp.float32).astype(jnp.bfloat16), 'tp', sc...  61.6 us
    ppermute x6, waiting for transfers between devices, on_device(): lax.ppermute(ring[-1], 'tp', [(dev, (dev + 1) % 4) for dev in range(4)])  51.3 us
    all_gather x1, waiting for transfers between devices, on_device(): lax.all_gather(w_value, 'sp', axis=1, tiled=True)  43 us
    dot_general x2, matrix products, on_device(): jnp.dot(gated, layer_output, preferred_element_type=jnp.float32)  14.3 us
    reduce_sum x2, other arithmetic, on_device(): jnp.mean(row_float * row_float, axis=-1, keepdims=True) + EPSILON  11.5 us
  transfers between devices with their start and end apart: 14, of which 14 were waited for; matrix products, arithmetic and copies ran while one was open for 3% of the time, Pallas kernels for 0%

profile of v1, /device:TPU:0, one launch (start us, length us, event | category | flops | bytes accessed | tf_op | source)
XLA Modules:
  0.0 434.2 jit_solution(15407300332681604105)
XLA Ops:
  6.5 0.7 all-gather.9.cloned.1.call-update
  7.3 0.7 all-gather.7.cloned.1.call-update
  9.9 9.0 %collective-permute-done = bf16[512,512]{1,0:T(8,128)(2,1)S(1)} collective-permute-done((bf16[512,512]{1,0:T(8,128)(2,1)}, bf16[512,512]{1,0:T(8,128)(2,1)S(1)}, u32[]{:S(2)}, u32[]{:S(2)}) %collective-permute-start) | collective-permute-done | bytes 524320 | tf_op jit(solution)/shard_map/ppermute | solution.py:31
  19.0 8.6 %collective-permute-done.1 = bf16[512,512]{1,0:T(8,128)(2,1)S(1)} collective-permute-done((bf16[512,512]{1,0:T(8,128)(2,1)S(1)}, bf16[512,512]{1,0:T(8,128)(2,1)S(1)}, u32[]{:S(2)}, u32[]{:S(2)}) %collective-permute-start.1) | collective-permute-done | bytes 524320 | tf_op jit(solution)/shard_map/ppermute | solution.py:31
  27.5 0.8 fusion.54
  28.4 7.9 %collective-permute-done.2 = bf16[512,512]{1,0:T(8,128)(2,1)} collective-permute-done((bf16[512,512]{1,0:T(8,128)(2,1)S(1)}, bf16[512,512]{1,0:T(8,128)(2,1)}, u32[]{:S(2)}, u32[]{:S(2)}) %collective-permute-start.2) | collective-permute-done | bytes 524320 | tf_op jit(solution)/shard_map/ppermute | solution.py:31
  36.2 5.8 %fusion = (f32[512]{0:T(512)S(1)}, bf16[512,2048]{1,0:T(8,128)(2,1)S(1)}) fusion(s32[]{:T(128)S(6)} %select_n.13, bf16[512,512]{1,0:T(8,128)(2,1)} %param.9, bf16[512,512]{1,0:T(8,128)(2,1)S(1)} %collective-permute-done, bf16[512,512]{1,0:T(8,128)(2,1)S(1)} %collective-permute-done.1, bf16[512,512]{1,0:T(8,128)(2,1)} %collective-permute-done.2), kind=kLoop, calls=%fused_computation.4 | loop fusion | flops 19922432 | bytes 4196356 | tf_op jit(solution)/shard_map/reduce_sum | solution.py:38
  42.1 43.0 %all-gather.9.cloned.1.call-done = bf16[2,2048,512]{2,1,0:T(8,128)(2,1)} async-done(((bf16[2,256,512]{2,1,0:T(8,128)(2,1)}), bf16[2,2048,512]{2,1,0:T(8,128)(2,1)}) %all-gather.9.cloned.1.call-update) | async-done | bytes 4194320 | tf_op jit(solution)/shard_map/all_gather | solution.py:18
  85.0 3.9 fusion.23
  88.9 69.6 %all-gather.7.cloned.1.call-done = bf16[2,2048,512]{2,1,0:T(8,128)(2,1)} async-done(((bf16[2,256,512]{2,1,0:T(8,128)(2,1)}), bf16[2,2048,512]{2,1,0:T(8,128)(2,1)}) %all-gather.7.cloned.1.call-update) | async-done | bytes 4194320 | tf_op jit(solution)/shard_map/all_gather | solution.py:19
  158.6 3.2 fusion.32
  161.7 2.5 collective-permute-start.3
  164.2 1.3 collective-permute-done.3
  165.5 1.1 maximum_convert_fusion
  166.7 65.5 %all-gather.5.cloned.1.call-done = bf16[2,2048,512]{2,1,0:T(8,128)(2,1)} async-done(((bf16[2,256,512]{2,1,0:T(8,128)(2,1)}), bf16[2,2048,512]{2,1,0:T(8,128)(2,1)}) %all-gather.5.cloned.1.call-update) | async-done | bytes 4194320 | tf_op jit(solution)/shard_map/all_gather | solution.py:20
  232.1 75.1 %all-gather.11.cloned.1.call-done = bf16[2,512,2048]{2,1,0:T(8,128)(2,1)} async-done(((bf16[2,512,256]{2,1,0:T(8,128)(2,1)}), bf16[2,512,2048]{2,1,0:T(8,128)(2,1)}) %all-gather.11.cloned.1.call-update) | async-done | bytes 4194320 | tf_op jit(solution)/shard_map/all_gather | solution.py:22
  307.2 7.1 %convolution_convert_fusion.1 = bf16[512,2048]{1,0:T(8,128)(2,1)} fusion(bf16[2,512,2048]{2,1,0:T(8,128)(2,1)} %all-gather.11.cloned.1.call-done, bf16[2,2048,512]{2,1,0:T(8,128)(2,1)} %all-gather.5.cloned.1.call-done, f32[514,512]{1,0:T(8,128)} %maximum_convert_fusion, f32[512]{0:T(512)S(1)} %bitcast.61, f32[512]{0:T(512)S(1)} %bitcast.62, ...), kind=kOutput, calls=%fused_computation.27 | convolution fusion | flops 2154561536 | bytes 11550720 | tf_op jit(solution)/shard_map/dot_general | solution.py:54
  314.4 29.5 %reduce-scatter.3.cloned.1.call-done = bf16[512,512]{1,0:T(8,128)(2,1)} async-done(((bf16[512,2048]{1,0:T(8,128)(2,1)}), bf16[512,512]{1,0:T(8,128)(2,1)}) %reduce-scatter.3.cloned.1.call-update) | async-done | bytes 524304 | tf_op jit(solution)/shard_map/reduce_scatter | solution.py:57
  343.9 1.3 add_convert_fusion.1
  345.3 8.6 %collective-permute-done.4 = bf16[512,512]{1,0:T(8,128)(2,1)S(1)} collective-permute-done((bf16[512,512]{1,0:T(8,128)(2,1)S(1)}, bf16[512,512]{1,0:T(8,128)(2,1)S(1)}, u32[]{:S(2)}, u32[]{:S(2)}) %collective-permute-start.4) | collective-permute-done | bytes 524320 | tf_op jit(solution)/shard_map/ppermute | solution.py:31
  353.9 8.6 %collective-permute-done.5 = bf16[512,512]{1,0:T(8,128)(2,1)S(1)} collective-permute-done((bf16[512,512]{1,0:T(8,128)(2,1)S(1)}, bf16[512,512]{1,0:T(8,128)(2,1)S(1)}, u32[]{:S(2)}, u32[]{:S(2)}) %collective-permute-start.5) | collective-permute-done | bytes 524320 | tf_op jit(solution)/shard_map/ppermute | solution.py:31
  362.5 8.6 %collective-permute-done.6 = bf16[512,512]{1,0:T(8,128)(2,1)S(1)} collective-permute-done((bf16[512,512]{1,0:T(8,128)(2,1)S(1)}, bf16[512,512]{1,0:T(8,128)(2,1)S(1)}, u32[]{:S(2)}, u32[]{:S(2)}) %collective-permute-start.6) | collective-permute-done | bytes 524320 | tf_op jit(solution)/shard_map/ppermute | solution.py:31
  371.1 5.7 %fusion.3 = (f32[512]{0:T(512)S(1)}, bf16[512,2048]{1,0:T(8,128)(2,1)S(1)}) fusion(s32[]{:T(128)S(6)} %select_n.13, bf16[512,512]{1,0:T(8,128)(2,1)S(1)} %add_convert_fusion.1, bf16[512,512]{1,0:T(8,128)(2,1)S(1)} %collective-permute-done.4, bf16[512,512]{1,0:T(8,128)(2,1)S(1)} %collective-permute-done.5, bf16[512,512]{1,0:T(8,128)(2,1)S(1)} %collective-permute-done.6), kind=kLoop, calls=%fused_computation.7 | loop fusion | flops 19922432 | bytes 4196356 | tf_op jit(solution)/shard_map/reduce_sum | solution.py:38
  376.8 1.3 fusion.20
  378.1 0.9 copy-done.3
  379.0 1.3 fusion.30
  380.3 3.4 collective-permute-start.7
  383.7 1.3 collective-permute-done.7
  385.0 1.1 maximum_convert_fusion.1
  386.1 7.2 %convolution_convert_fusion = bf16[512,2048]{1,0:T(8,128)(2,1)} fusion(bf16[2,512,2048]{2,1,0:T(8,128)(2,1)} %all-gather.11.cloned.1.call-done, bf16[2,2048,512]{2,1,0:T(8,128)(2,1)} %all-gather.5.cloned.1.call-done, f32[514,512]{1,0:T(8,128)} %maximum_convert_fusion.1, f32[512]{0:T(512)S(1)} %bitcast.59, f32[512]{0:T(512)S(1)} %bitcast.60, ...), kind=kOutput, calls=%fused_computation.26 | convolution fusion | flops 2154561536 | bytes 11550720 | tf_op jit(solution)/shard_map/dot_general | solution.py:54
  393.3 32.1 %reduce-scatter.5.cloned.1.call-done = bf16[512,512]{1,0:T(8,128)(2,1)} async-done(((bf16[512,2048]{1,0:T(8,128)(2,1)}), bf16[512,512]{1,0:T(8,128)(2,1)}) %reduce-scatter.5.cloned.1.call-update) | async-done | bytes 524304 | tf_op jit(solution)/shard_map/reduce_scatter | solution.py:57
  425.4 2.0 add_convert_fusion
  (28 shorter events, 2.1 us)
Async XLA Ops:
  6.5 78.5 %all-gather.9.cloned.1.call-start = ((), (), s32[]{:S(2)}) async-start(), calls=%async_computation.4 | async-start | bytes 4718592 | tf_op jit(solution)/shard_map/all_gather | solution.py:18
  7.3 151.3 %all-gather.7.cloned.1.call-start = ((), (), s32[]{:S(2)}) async-start(), calls=%async_computation.3 | async-start | bytes 4718592 | tf_op jit(solution)/shard_map/all_gather | solution.py:19
  8.0 224.1 %all-gather.5.cloned.1.call-start = ((), (), s32[]{:S(2)}) async-start(), calls=%async_computation.2 | async-start | bytes 4718592 | tf_op jit(solution)/shard_map/all_gather | solution.py:20
  8.7 298.5 %all-gather.11.cloned.1.call-start = ((), (), s32[]{:S(2)}) async-start(), calls=%async_computation.5 | async-start | bytes 4718592 | tf_op jit(solution)/shard_map/all_gather | solution.py:22
  9.3 334.6 %reduce-scatter.3.cloned.1.call-start = ((), (), s32[]{:S(2)}) async-start(), calls=%async_computation.6 | async-start | bytes 2621440 | tf_op jit(solution)/shard_map/reduce_scatter | solution.py:57
  9.4 9.6 %collective-permute-start = (bf16[512,512]{1,0:T(8,128)(2,1)}, bf16[512,512]{1,0:T(8,128)(2,1)S(1)}, u32[]{:S(2)}, u32[]{:S(2)}) collective-permute-start(bf16[512,512]{1,0:T(8,128)(2,1)} %param.9), channel_id=1, source_target_pairs={{0,1},{1,2},{2,3},{3,0},{4,5},{5,6},{6,7},{7,4},{8,9},{9,10},{10,1... | collective-permute-start | bytes 1572872 | tf_op jit(solution)/shard_map/ppermute | solution.py:31
  18.9 8.6 %collective-permute-start.1 = (bf16[512,512]{1,0:T(8,128)(2,1)S(1)}, bf16[512,512]{1,0:T(8,128)(2,1)S(1)}, u32[]{:S(2)}, u32[]{:S(2)}) collective-permute-start(bf16[512,512]{1,0:T(8,128)(2,1)S(1)} %collective-permute-done), channel_id=1, source_target_pairs={{0,1},{1,2},{2,3},{3,0},{4,5},{5,6},{6,7},{7,4},{8,9},{9,10},{10,1... | collective-permute-start | bytes 1572872 | tf_op jit(solution)/shard_map/ppermute | solution.py:31
  27.5 8.7 %collective-permute-start.2 = (bf16[512,512]{1,0:T(8,128)(2,1)S(1)}, bf16[512,512]{1,0:T(8,128)(2,1)}, u32[]{:S(2)}, u32[]{:S(2)}) collective-permute-start(bf16[512,512]{1,0:T(8,128)(2,1)S(1)} %collective-permute-done.1), channel_id=1, source_target_pairs={{0,1},{1,2},{2,3},{3,0},{4,5},{5,6},{6,7},{7,4},{8,9},{9,10},{10,1... | collective-permute-start | bytes 1572872 | tf_op jit(solution)/shard_map/ppermute | solution.py:31
  88.9 75.3 %copy-start.1 = (f32[2,3,512]{2,0,1:T(2,128)S(1)}, f32[2,3,512]{2,0,1:T(2,128)}, u32[]{:S(2)}) copy-start(f32[2,3,512]{2,0,1:T(2,128)} %param.14) | copy-start | bytes 36868
  161.7 3.8 collective-permute-start.3
  307.2 36.7 %copy-start = (bf16[512,512]{1,0:T(8,128)(2,1)S(1)}, bf16[512,512]{1,0:T(8,128)(2,1)}, u32[]{:S(2)}) copy-start(bf16[512,512]{1,0:T(8,128)(2,1)} %param.9) | copy-start | bytes 1572868
  314.4 111.1 %reduce-scatter.5.cloned.1.call-start = ((), (), s32[]{:S(2)}) async-start(), calls=%async_computation.7 | async-start | bytes 2621440 | tf_op jit(solution)/shard_map/reduce_scatter | solution.py:57
  343.9 32.9 %copy-start.2 = (bf16[2,2048,512]{2,1,0:T(8,128)(2,1)S(1)}, bf16[2,2048,512]{2,1,0:T(8,128)(2,1)}, u32[]{:S(2)}) copy-start(bf16[2,2048,512]{2,1,0:T(8,128)(2,1)} %all-gather.9.cloned.1.call-done) | copy-start | bytes 12582916
  345.2 8.7 %collective-permute-start.4 = (bf16[512,512]{1,0:T(8,128)(2,1)S(1)}, bf16[512,512]{1,0:T(8,128)(2,1)S(1)}, u32[]{:S(2)}, u32[]{:S(2)}) collective-permute-start(bf16[512,512]{1,0:T(8,128)(2,1)S(1)} %add_convert_fusion.1), channel_id=1, source_target_pairs={{0,1},{1,2},{2,3},{3,0},{4,5},{5,6},{6,7},{7,4},{8,9},{9,10},{10,1... | collective-permute-start | bytes 1572872 | tf_op jit(solution)/shard_map/ppermute | solution.py:31
  353.9 8.6 %collective-permute-start.5 = (bf16[512,512]{1,0:T(8,128)(2,1)S(1)}, bf16[512,512]{1,0:T(8,128)(2,1)S(1)}, u32[]{:S(2)}, u32[]{:S(2)}) collective-permute-start(bf16[512,512]{1,0:T(8,128)(2,1)S(1)} %collective-permute-done.4), channel_id=1, source_target_pairs={{0,1},{1,2},{2,3},{3,0},{4,5},{5,6},{6,7},{7,4},{8,9},{9,10},{10,1... | collective-permute-start | bytes 1572872 | tf_op jit(solution)/shard_map/ppermute | solution.py:31
  362.5 8.6 %collective-permute-start.6 = (bf16[512,512]{1,0:T(8,128)(2,1)S(1)}, bf16[512,512]{1,0:T(8,128)(2,1)S(1)}, u32[]{:S(2)}, u32[]{:S(2)}) collective-permute-start(bf16[512,512]{1,0:T(8,128)(2,1)S(1)} %collective-permute-done.5), channel_id=1, source_target_pairs={{0,1},{1,2},{2,3},{3,0},{4,5},{5,6},{6,7},{7,4},{8,9},{9,10},{10,1... | collective-permute-start | bytes 1572872 | tf_op jit(solution)/shard_map/ppermute | solution.py:31
  376.8 2.2 copy-start.3
  380.3 4.7 %collective-permute-start.7 = (bf16[2,512]{1,0:T(2,128)(2,1)S(1)}, bf16[2,512]{1,0:T(2,128)(2,1)S(1)}, u32[]{:S(2)}, u32[]{:S(2)}) collective-permute-start(bf16[2,512]{1,0:T(2,128)(2,1)S(1)} %slice.121), channel_id=1, source_target_pairs={{0,4},{4,8},{8,12},{12,16},{16,20},{20,24},{24,28},{1,5},{5,9},{9,... | collective-permute-start | bytes 6152 | tf_op jit(solution)/shard_map/ppermute | solution.py:13
Sparse Core Ops, SparseCore 0:
  9.5 75.4 all-gather.8
  87.2 71.2 all-gather.6
  160.8 71.2 all-gather.4
  234.0 73.1 all-gather.10
  314.5 29.3 reduce-scatter.2
  393.4 31.9 reduce-scatter.4
